TPU v7x, 32 devices: a whole 2x2x4 slice. The times are simulated.
32 devices in a mesh: kv: 8 (over y, x, core), tp: 4 (over z).
Axes of the slice: x: 2, y: 2, z: 4, core: 2. Of those that a mesh axis runs over, the one named last changes fastest.
Arguments:
- tokens: bfloat16 [64, 4, 4096], P(None, None, ('kv', 'tp')), may hold values from -36 to 36
- lengths: int32 [64], replicated, may hold values from 1 to 4, 112 in all
- state: float32 [64, 128, 4096], P('kv', None, 'tp'), may hold values from -0.6 to 0.6
- attn_gain: float32 [4096], P('kv'), may hold values from 0.1 to 1.9
- w_query: bfloat16 [4096, 4096], P('kv', 'tp'), may hold values from -0.09375 to 0.09375
- w_key: bfloat16 [4096, 4096], P('kv', 'tp'), may hold values from -0.09375 to 0.09375
- w_value: bfloat16 [4096, 4096], P('kv', 'tp'), may hold values from -0.09375 to 0.09375
- w_beta: bfloat16 [4096, 32], replicated, may hold values from -0.09375 to 0.09375
- w_alpha: bfloat16 [4096, 32], replicated, may hold values from -0.09375 to 0.09375
- decay_rate: float32 [32], replicated, may hold values from 0.05 to 3
- decay_bias: float32 [32], replicated, may hold values from -3 to 3
- out_gain: float32 [128], replicated, may hold values from 0.1 to 1.9
- w_out: bfloat16 [4096, 4096], P('tp', 'kv'), may hold values from -0.09375 to 0.09375
- mix_gain: float32 [4096], P('kv'), may hold values from 0.1 to 1.9
- w_gate: bfloat16 [4096, 11008], P('kv', 'tp'), may hold values from -0.09375 to 0.09375
- w_up: bfloat16 [4096, 11008], P('kv', 'tp'), may hold values from -0.09375 to 0.09375
- w_down: bfloat16 [11008, 4096], P('tp', 'kv'), may hold values from -0.0546875 to 0.0546875
Outputs:
- mixed: bfloat16 [64, 4, 4096], P(None, None, ('kv', 'tp'))
- new_state: float32 [64, 128, 4096], P('kv', None, 'tp')
Inputs may be any that keep to these rules, and one draw needn't show every extreme that they name: Each sequence has 1 to 4 live tokens, the first ones of its block, and the lengths sum to 112.
All inputs are finite; a program needn't handle non-finite values.
Results may differ from a plain program's by a relative error of at most 0.015.
Values may be sent and summed in bfloat16 or wider, within the bound.
A program may use at most 64 MiB of HBM per device.

v0:
```python
import jax
import jax.numpy as jnp
from jax import lax
from jax.experimental import pallas as pl
from jax.experimental.pallas import tpu as pltpu
from jax.sharding import PartitionSpec as P

MESH = pl.DeviceIdType.MESH
F32 = jnp.float32
BF16 = jnp.bfloat16

D = 4096
HEAD_DIM = 128


EPSILON = 1e-06


def unit_rows(vectors):
    return vectors * lax.rsqrt(jnp.sum(vectors * vectors, axis=-1, keepdims=True) + EPSILON)


def delta_block(queries, unit_keys, values_split, beta, log_decay, carried):
    highest = lax.Precision.HIGHEST
    seq_count, span_len, heads_here = beta.shape
    cumulative = jnp.cumsum(log_decay, axis=1)
    position = jnp.arange(span_len)
    inclusive = (position[:, None] >= position[None, :])[None, :, :, None]
    strict = (position[:, None] > position[None, :])[None, :, :, None]
    gap_matrix = cumulative[:, :, None, :] - cumulative[:, None, :, :]
    decay_matrix = jnp.where(inclusive, jnp.exp(jnp.where(inclusive, gap_matrix, 0.0)), 0.0)
    key_dots = jnp.einsum("nihd,njhd->nijh", unit_keys, unit_keys, precision=highest)
    query_dots = jnp.einsum("nihd,njhd->nijh", queries, unit_keys, precision=highest) * decay_matrix
    lower_part = jnp.where(strict, key_dots * decay_matrix * beta[:, :, None, :], 0.0)
    identity = jnp.eye(span_len, dtype=jnp.float32)
    inverse_rows = []
    for step in range(span_len):
        row_now = jnp.broadcast_to(identity[step][None, :, None], (seq_count, span_len, heads_here))
        for prior in range(step):
            row_now = row_now - lower_part[:, step, prior, :][:, None, :] * inverse_rows[prior]
        inverse_rows.append(row_now)
    inverse = jnp.stack(inverse_rows, axis=1)
    beta_value = beta[..., None] * values_split
    beta_key = (beta * jnp.exp(cumulative))[..., None] * unit_keys
    base_update = jnp.einsum("nich,nche->nihe", inverse, beta_value, precision=highest)
    key_weights = jnp.einsum("nich,nchd->nihd", inverse, beta_key, precision=highest)
    corrected = base_update - jnp.einsum("nihd,ndhe->nihe", key_weights, carried, precision=highest)
    decayed_queries = queries * jnp.exp(cumulative)[..., None]
    attended = jnp.einsum("nihd,ndhe->nihe", decayed_queries, carried, precision=highest)
    attended = attended + jnp.einsum("nijh,njhe->nihe", query_dots, corrected, precision=highest)
    block_total = cumulative[:, -1, :]
    key_tail = unit_keys * jnp.exp(block_total[:, None, :] - cumulative)[..., None]
    updated = carried * jnp.exp(block_total)[:, None, :, None]
    updated = updated + jnp.einsum("nihd,nihe->ndhe", key_tail, corrected, precision=highest)
    return (attended, updated)


def body(
    tokens,
    lengths,
    state,
    attn_gain,
    w_query,
    w_key,
    w_value,
    w_beta,
    w_alpha,
    decay_rate,
    decay_bias,
    out_gain,
    w_out,
    mix_gain,
    w_gate,
    w_up,
    w_down,
):
    kv_index = lax.axis_index("kv")
    tp_index = lax.axis_index("tp")
    kv_count = lax.axis_size("kv")
    batch_all, span_len, own_cols = tokens.shape
    row_count = batch_all * span_len
    seq_count = state.shape[0]
    local_rows = seq_count * span_len
    head_size = state.shape[1]
    heads_here = state.shape[2] // head_size
    block_width = attn_gain.shape[0]
    flat_rows = tokens.reshape(row_count, own_cols)
    live_all = (jnp.arange(span_len, dtype=jnp.int32)[None, :] < lengths[:, None]).reshape(
        row_count, 1
    )
    gathered = lax.all_gather(flat_rows, "tp", axis=1, tiled=True).astype(jnp.float32)
    squares_in = jnp.sum(gathered * gathered, axis=1)
    normed_in = (gathered * attn_gain).astype(jnp.bfloat16)
    beta_rows = lax.dynamic_slice_in_dim(w_beta, kv_index * block_width, block_width, 0)
    alpha_rows = lax.dynamic_slice_in_dim(w_alpha, kv_index * block_width, block_width, 0)
    query_part = jnp.dot(normed_in, w_query, preferred_element_type=jnp.float32)
    key_part = jnp.dot(normed_in, w_key, preferred_element_type=jnp.float32)
    value_part = jnp.dot(normed_in, w_value, preferred_element_type=jnp.float32)
    beta_part = jnp.dot(normed_in, beta_rows, preferred_element_type=jnp.float32)
    alpha_part = jnp.dot(normed_in, alpha_rows, preferred_element_type=jnp.float32)
    squares_all = lax.psum(squares_in, "kv")
    squares_own = lax.dynamic_slice_in_dim(squares_all, kv_index * local_rows, local_rows, 0)
    query_sum, key_sum, value_sum, beta_sum, alpha_sum = (
        lax.psum_scatter(
            query_part.astype(jnp.bfloat16), "kv", scatter_dimension=0, tiled=True
        ).astype(jnp.float32),
        lax.psum_scatter(
            key_part.astype(jnp.bfloat16), "kv", scatter_dimension=0, tiled=True
        ).astype(jnp.float32),
        lax.psum_scatter(
            value_part.astype(jnp.bfloat16), "kv", scatter_dimension=0, tiled=True
        ).astype(jnp.float32),
        lax.psum_scatter(
            beta_part.astype(jnp.bfloat16), "kv", scatter_dimension=0, tiled=True
        ).astype(jnp.float32),
        lax.psum_scatter(
            alpha_part.astype(jnp.bfloat16), "kv", scatter_dimension=0, tiled=True
        ).astype(jnp.float32),
    )
    row_scale = lax.rsqrt(squares_own / D + EPSILON)[:, None]
    head_start = tp_index * heads_here
    lengths_own = lax.dynamic_slice_in_dim(lengths, kv_index * seq_count, seq_count, 0)
    live_own = (jnp.arange(span_len, dtype=jnp.int32)[None, :] < lengths_own[:, None])[..., None]
    beta_heads = lax.dynamic_slice_in_dim(beta_sum, head_start, heads_here, 1) * row_scale
    alpha_heads = lax.dynamic_slice_in_dim(alpha_sum, head_start, heads_here, 1) * row_scale
    rate_here = lax.dynamic_slice_in_dim(decay_rate, head_start, heads_here, 0)
    bias_here = lax.dynamic_slice_in_dim(decay_bias, head_start, heads_here, 0)
    beta = jnp.where(
        live_own, jax.nn.sigmoid(beta_heads).reshape(seq_count, span_len, heads_here), 0.0
    )
    log_decay = -rate_here * jax.nn.softplus(alpha_heads + bias_here)
    log_decay = jnp.where(live_own, log_decay.reshape(seq_count, span_len, heads_here), 0.0)
    split_shape = (seq_count, span_len, heads_here, head_size)
    queries = unit_rows((query_sum * row_scale).reshape(split_shape)) * HEAD_DIM ** (-0.5)
    unit_keys = unit_rows((key_sum * row_scale).reshape(split_shape))
    values_split = (value_sum * row_scale).reshape(split_shape)
    carried = state.reshape(seq_count, head_size, heads_here, head_size)
    attended, updated = delta_block(queries, unit_keys, values_split, beta, log_decay, carried)
    head_out = (
        attended
        * lax.rsqrt(jnp.mean(attended * attended, axis=-1, keepdims=True) + EPSILON)
        * out_gain
    )
    head_out = head_out.astype(jnp.bfloat16).reshape(local_rows, heads_here * head_size)
    pack_rows = min((batch_all * 7 // 4 + kv_count - 1) // kv_count * kv_count, row_count)
    live_flat = live_all.reshape(row_count).astype(jnp.int32)
    slot_index = jnp.cumsum(live_flat) - 1
    picker = (
        (slot_index[None, :] == jnp.arange(pack_rows, dtype=jnp.int32)[:, None])
        & (live_flat[None, :] > 0)
    ).astype(jnp.bfloat16)
    heads_every = lax.all_gather(head_out, "kv", axis=0, tiled=True)
    packed_heads = jnp.dot(picker, heads_every, preferred_element_type=jnp.float32).astype(
        jnp.bfloat16
    )
    attn_part = jnp.dot(packed_heads, w_out, preferred_element_type=jnp.float32)
    base_rows = jnp.dot(picker, flat_rows, preferred_element_type=jnp.float32)
    attn_own = lax.psum_scatter(
        attn_part.astype(jnp.bfloat16), "tp", scatter_dimension=1, tiled=True
    ).astype(jnp.float32)
    middle = (base_rows + attn_own).astype(jnp.bfloat16)
    middle_rows = lax.all_gather(middle, "tp", axis=1, tiled=True).astype(jnp.float32)
    squares_mid = jnp.sum(middle_rows * middle_rows, axis=1)
    normed_mid = (middle_rows * mix_gain).astype(jnp.bfloat16)
    gate_part = jnp.dot(normed_mid, w_gate, preferred_element_type=jnp.float32)
    up_part = jnp.dot(normed_mid, w_up, preferred_element_type=jnp.float32)
    squares_total = lax.psum(squares_mid, "kv")
    gate_sum, up_sum = (
        lax.psum(gate_part.astype(jnp.bfloat16), "kv").astype(jnp.float32),
        lax.psum(up_part.astype(jnp.bfloat16), "kv").astype(jnp.float32),
    )
    mid_scale = lax.rsqrt(squares_total / D + EPSILON)[:, None]
    hidden = (jax.nn.silu(gate_sum * mid_scale) * (up_sum * mid_scale)).astype(jnp.bfloat16)
    down_part = jnp.dot(hidden, w_down, preferred_element_type=jnp.float32)
    down_own = lax.psum_scatter(
        down_part.astype(jnp.bfloat16), "tp", scatter_dimension=1, tiled=True
    ).astype(jnp.float32)
    result_rows = middle.astype(jnp.float32) + down_own
    result_rows = jnp.dot(
        picker.astype(jnp.float32).T,
        result_rows,
        precision=lax.Precision.HIGHEST,
        preferred_element_type=jnp.float32,
    )
    mixed = (
        jnp.where(live_all, result_rows, 0.0)
        .astype(jnp.bfloat16)
        .reshape(batch_all, span_len, own_cols)
    )
    return (mixed, updated.reshape(seq_count, head_size, heads_here * head_size))


def iota(shape, axis):
    return lax.broadcasted_iota(jnp.int32, shape, axis)


def dot(a, b):
    return jnp.dot(a, b, preferred_element_type=F32)


def dot_t(a, b):
    return lax.dot_general(a, b, (((1,), (1,)), ((), ())), preferred_element_type=F32)


def dot_exact(a, b):
    return jnp.dot(a, b, precision=lax.Precision.HIGHEST, preferred_element_type=F32)


def head_sum(x, heads, size):
    pieces = []
    for h in range(heads):
        total = jnp.sum(x[:, h * size : (h + 1) * size], axis=1, keepdims=True)
        pieces.append(jnp.broadcast_to(total, (x.shape[0], size)))
    return jnp.concatenate(pieces, axis=1)


def high_low(x):
    high = x.astype(BF16)
    return high.astype(F32), x - high.astype(F32)


def layer_kernel(
    dims,
    tokens_ref,
    lengths_ref,
    state_hbm,
    attn_gain_ref,
    wq_hbm,
    wk_hbm,
    wv_hbm,
    wb_hbm,
    wa_hbm,
    rate_ref,
    bias_ref,
    out_gain_ref,
    wo_hbm,
    mix_gain_ref,
    wg_hbm,
    wu_hbm,
    wd_hbm,
    mixed_ref,
    new_state_hbm,
    state,
    w_qkv,
    w_beta,
    w_alpha,
    w_out,
    w_gate,
    w_up,
    w_down,
    tok_all,
    qkv_part,
    qkv_pair,
    qkv_red,
    qkv_recv,
    head_all,
    attn_part,
    attn_recv,
    mid_all,
    gu_part,
    gu_pair,
    gu_red,
    gu_recv,
    hid_first,
    hid_second,
    down_part,
    down_recv,
    placed_ref,
    square_ref,
    normed_ref,
    side_ref,
    load_sem,
    store_sem,
    tp_send,
    tp_recv,
    pair_send,
    pair_recv,
    chip_send,
    chip_recv,
    fwd_send,
    fwd_recv,
):
    n_kv, n_tp, batch, span, seqs, heads, size, width, ff, rows, packs, unit = dims
    chips = n_kv // 2
    kv = lax.axis_index("kv")
    tp = lax.axis_index("tp")
    core = lax.rem(kv, 2)
    chip = kv // 2
    other = 1 - core
    partner = chip * 2 + other
    slots = batch * span
    local = seqs * span
    vw = heads * size

    def chip_at(d):
        return lax.rem(chip + d, chips)

    def chip_from(d):
        return lax.rem(chip + chips - d, chips)

    loads = [
        pltpu.make_async_copy(wq_hbm, w_qkv.at[0], load_sem.at[0]),
        pltpu.make_async_copy(wk_hbm, w_qkv.at[1], load_sem.at[1]),
        pltpu.make_async_copy(wv_hbm, w_qkv.at[2], load_sem.at[2]),
        pltpu.make_async_copy(
            wb_hbm.at[:, pl.ds(pl.multiple_of(kv * width, width), width)], w_beta, load_sem.at[3]
        ),
        pltpu.make_async_copy(
            wa_hbm.at[:, pl.ds(pl.multiple_of(kv * width, width), width)], w_alpha, load_sem.at[4]
        ),
        pltpu.make_async_copy(state_hbm, state, load_sem.at[5]),
        pltpu.make_async_copy(wo_hbm, w_out, load_sem.at[6]),
        pltpu.make_async_copy(wg_hbm, w_gate, load_sem.at[7]),
        pltpu.make_async_copy(wu_hbm, w_up, load_sem.at[8]),
        pltpu.make_async_copy(wd_hbm, w_down, load_sem.at[9]),
    ]
    for load in loads:
        load.start()

    barrier = pltpu.get_barrier_semaphore()
    pl.semaphore_signal(barrier, inc=1, device_id={"kv": partner}, device_id_type=MESH)
    for d in range(1, chips):
        pl.semaphore_signal(
            barrier, inc=1, device_id={"kv": chip_at(d) * 2 + core}, device_id_type=MESH
        )
    for d in range(1, n_tp):
        pl.semaphore_signal(
            barrier, inc=1, device_id={"tp": lax.rem(tp + d, n_tp)}, device_id_type=MESH
        )

    lengths_row = lengths_ref[...].astype(F32)
    spread = (iota((batch, slots), 1) // span == iota((batch, slots), 0)).astype(BF16)
    length_of = dot(jnp.broadcast_to(lengths_row, (8, batch)).astype(BF16), spread)
    live_row = (lax.rem(iota((8, slots), 1), span).astype(F32) < length_of).astype(F32)
    before = (iota((slots, slots), 0) < iota((slots, slots), 1)).astype(BF16)
    slot_row = dot(live_row.astype(BF16), before)
    slot_row = jnp.where(live_row > 0.0, slot_row, -1.0)[0:1, :]
    picker = (iota((packs, slots), 0).astype(F32) == slot_row).astype(BF16)
    position = iota((slots, slots), 1) // local
    inner = lax.rem(iota((slots, slots), 1), local)
    from_slot = (
        (lax.rem(position, chips) * 2 + position // chips) * seqs + lax.rem(inner, seqs)
    ) * span + inner // seqs
    order = (iota((slots, slots), 0) == from_slot).astype(BF16)
    picker_kv = dot(picker, order).astype(BF16)

    own_tokens = dot(picker, tokens_ref[...])
    tok_all[tp] = own_tokens.astype(BF16)
    pl.semaphore_wait(barrier, 1 + (chips - 1) + (n_tp - 1))

    def tp_copies(phase, source_at, dest_at):
        copies = []
        for d in range(1, n_tp):
            peer = lax.rem(tp + d, n_tp)
            copies.append(
                pltpu.make_async_remote_copy(
                    src_ref=source_at(peer, d),
                    dst_ref=dest_at(peer, d),
                    send_sem=tp_send.at[phase, d - 1],
                    recv_sem=tp_recv.at[phase, d - 1],
                    device_id={"tp": peer},
                    device_id_type=MESH,
                )
            )
        return copies

    def exchange_start(copies):
        for copy in copies:
            copy.start()

    def exchange_wait(copies):
        for copy in copies:
            copy.wait()

    copies = tp_copies(0, lambda peer, d: tok_all.at[tp], lambda peer, d: tok_all.at[tp])
    exchange_start(copies)
    exchange_wait(copies)
    gathered = jnp.concatenate([tok_all[j] for j in range(n_tp)], axis=1).astype(F32)
    squares = jnp.sum(gathered * gathered, axis=1, keepdims=True)
    normed = (gathered * attn_gain_ref[...]).astype(BF16)
    square_high, square_low = high_low(squares)
    square_pair = jnp.concatenate([square_high, square_low], axis=1).astype(BF16)

    def place(rows_packed):
        return lax.dot_general(
            picker_kv, rows_packed, (((0,), (0,)), ((), ())), preferred_element_type=F32
        ).astype(BF16)

    placed = place(normed)
    square_placed = place(square_pair)
    half = chips * local
    n_heads_all = wb_hbm.shape[0]
    qkv_width = 3 * vw + 128
    first = 128 + vw
    chunks = ((0, first), (first, first + vw), (first + vw, qkv_width))

    def halves(c, size_of):
        return pl.ds(pl.multiple_of(c * size_of, size_of), size_of)

    def pair_start(index, source, dest):
        copy = pltpu.make_async_remote_copy(
            src_ref=source,
            dst_ref=dest,
            send_sem=pair_send.at[index],
            recv_sem=pair_recv.at[index],
            device_id={"kv": partner},
            device_id_type=MESH,
        )
        copy.start()
        return copy

    def chip_start(index, d, source, dest):
        copy = pltpu.make_async_remote_copy(
            src_ref=source,
            dst_ref=dest,
            send_sem=chip_send.at[index, d - 1],
            recv_sem=chip_recv.at[index, d - 1],
            device_id={"kv": chip_at(d) * 2 + core},
            device_id_type=MESH,
        )
        copy.start()
        return copy

    placed_ref[...] = placed
    square_ref[...] = square_placed

    def qkv_chunk(m, c):
        part = halves(c, half)
        here = placed_ref[part, :]
        low, high = chunks[m]
        if m == 0:
            extra = jnp.concatenate(
                [
                    dot_t(here, w_beta[...]),
                    dot_t(here, w_alpha[...]),
                    square_ref[part, :].astype(F32),
                    jnp.zeros((half, 128 - 2 * n_heads_all - 2), F32),
                ],
                axis=1,
            )
            qkv_part[part, 0:128] = extra.astype(BF16)
            low = 128
        qkv_part[part, low:high] = dot(here, w_qkv[(1, 0, 2)[m]]).astype(BF16)

    def qkv_finish(m):
        pair_copies[m].wait()
        cols = slice(*chunks[m])
        for d in range(1, chips):
            dest = chip_at(d)
            at = halves(dest, local)
            mine = pl.ds(pl.multiple_of(core * half + dest * local, local), local)
            qkv_red[d - 1, :, cols] = (
                qkv_part[mine, cols].astype(F32) + qkv_pair[at, cols].astype(F32)
            ).astype(BF16)
            qkv_far[m].append(
                chip_start(m, d, qkv_red.at[d - 1, :, cols], qkv_recv.at[d - 1, :, cols])
            )

    pair_copies = []
    qkv_far = [[], [], []]
    for m in range(3):
        loads[(1, 0, 2)[m]].wait()
        if m == 0:
            loads[3].wait()
            loads[4].wait()
        qkv_chunk(m, other)
        cols = slice(*chunks[m])
        pair_copies.append(
            pair_start(m, qkv_part.at[halves(other, half), cols], qkv_pair.at[:, cols])
        )
        qkv_chunk(m, core)
        if m > 0:
            qkv_finish(m - 1)
    qkv_finish(2)

    loads[5].wait()
    state_low = state[...].reshape(seqs * size, vw).astype(BF16)

    def own_sum(m):
        exchange_wait(qkv_far[m])
        cols = slice(*chunks[m])
        at = halves(chip, local)
        mine = pl.ds(pl.multiple_of(core * half + chip * local, local), local)
        total = qkv_part[mine, cols].astype(F32) + qkv_pair[at, cols].astype(F32)
        for d in range(1, chips):
            total = total + qkv_recv[d - 1, :, cols].astype(F32)
        return total

    extra_keys = own_sum(0)
    extra = extra_keys[:, 0:128]
    lane = iota((local, 128), 1)
    sq_lane = (lane == 2 * n_heads_all) | (lane == 2 * n_heads_all + 1)
    sq_own = jnp.sum(jnp.where(sq_lane, extra, 0.0), axis=1, keepdims=True)
    row_scale = lax.rsqrt(sq_own / D + EPSILON)
    scaled_extra = jnp.where(sq_lane, 0.0, extra * row_scale)
    lane_of = iota((128, vw), 0)
    head_of = iota((128, vw), 1) // size + tp * heads
    beta_pre = dot_exact(scaled_extra, (lane_of == head_of).astype(F32))
    alpha_pre = dot_exact(scaled_extra, (lane_of == head_of + n_heads_all).astype(F32))
    per_head = (iota((n_heads_all, vw), 0) == iota((n_heads_all, vw), 1) // size + tp * heads).astype(F32)
    rate = dot_exact(jnp.broadcast_to(rate_ref[...], (8, n_heads_all)), per_head)[0:1, :]
    bias = dot_exact(jnp.broadcast_to(bias_ref[...], (8, n_heads_all)), per_head)[0:1, :]
    row_id = iota((local, batch), 0)
    seq_hit = iota((local, batch), 1) == kv * seqs + lax.rem(row_id, seqs)
    own_len = jnp.sum(jnp.where(seq_hit, lengths_row, 0.0), axis=1, keepdims=True)
    live = (iota((local, 1), 0) // seqs).astype(F32) < own_len
    beta = jnp.where(live, 1.0 / (1.0 + jnp.exp(-beta_pre)), 0.0)
    pre = alpha_pre + bias
    softplus = jnp.maximum(pre, 0.0) + jnp.log(1.0 + jnp.exp(-jnp.abs(pre)))
    log_decay = jnp.where(live, -rate * softplus, 0.0)

    k_raw = extra_keys[:, 128:] * row_scale
    keys = k_raw * lax.rsqrt(head_sum(k_raw * k_raw, heads, size) + EPSILON)
    q_raw = own_sum(1) * row_scale
    queries = q_raw * lax.rsqrt(head_sum(q_raw * q_raw, heads, size) + EPSILON) * size ** (-0.5)

    def token(x, t):
        return x[t * seqs : (t + 1) * seqs, :]

    cumulative = [token(log_decay, 0)]
    for t in range(1, span):
        cumulative.append(cumulative[-1] + token(log_decay, t))

    def blocked(x):
        keep = lax.rem(iota(x.shape, 0), seqs)
        return jnp.concatenate(
            [jnp.where(keep == n, x, 0.0).astype(BF16) for n in range(seqs)], axis=1
        )

    products = []
    for h in range(heads):
        cols = slice(h * size, (h + 1) * size)
        both = jnp.concatenate([keys[:, cols], queries[:, cols]], axis=0)
        products.append(dot(blocked(both), state_low[:, cols]))
    products = jnp.concatenate(products, axis=1)
    values = own_sum(2) * row_scale
    updates, attended = [], []
    for t in range(span):
        grown = jnp.exp(cumulative[t])
        update = token(values, t) - grown * token(products, t)
        for p in range(t):
            weight = jnp.exp(cumulative[t] - cumulative[p]) * head_sum(
                token(keys, t) * token(keys, p), heads, size
            )
            update = update - weight * updates[p]
        updates.append(token(beta, t) * update)
        result = grown * token(products, span + t)
        for p in range(t + 1):
            weight = jnp.exp(cumulative[t] - cumulative[p]) * head_sum(
                token(queries, t) * token(keys, p), heads, size
            )
            result = result + weight * updates[p]
        attended.append(result)
    attended = jnp.concatenate(attended, axis=0)
    gain = jnp.concatenate([out_gain_ref[...]] * heads, axis=1)
    head_out = attended * lax.rsqrt(head_sum(attended * attended, heads, size) / size + EPSILON) * gain

    def kv_gather_start(phase, buffer):
        spot = core * chips + chip
        own = pltpu.make_async_remote_copy(
            src_ref=buffer.at[spot],
            dst_ref=buffer.at[spot],
            send_sem=fwd_send.at[phase, 0],
            recv_sem=fwd_recv.at[phase, 0],
            device_id={"kv": partner},
            device_id_type=MESH,
        )
        far = [
            pltpu.make_async_remote_copy(
                src_ref=buffer.at[spot],
                dst_ref=buffer.at[spot],
                send_sem=chip_send.at[8 + phase, d - 1],
                recv_sem=chip_recv.at[8 + phase, d - 1],
                device_id={"kv": chip_at(d) * 2 + core},
                device_id_type=MESH,
            )
            for d in range(1, chips)
        ]
        exchange_start(far)
        own.start()
        return own, far

    def kv_gather_finish(phase, buffer, own, far):
        forwards = []
        for d in range(1, chips):
            far[d - 1].wait_recv()
            spot = core * chips + chip_from(d)
            forwards.append(
                pltpu.make_async_remote_copy(
                    src_ref=buffer.at[spot],
                    dst_ref=buffer.at[spot],
                    send_sem=fwd_send.at[phase, d],
                    recv_sem=fwd_recv.at[phase, d],
                    device_id={"kv": partner},
                    device_id_type=MESH,
                )
            )
            forwards[-1].start()
        own.wait()
        exchange_wait(forwards)
        for copy in far:
            copy.wait_send()

    head_all[core * chips + chip] = head_out.astype(BF16)
    own, far = kv_gather_start(0, head_all)

    final = cumulative[-1]
    tails = jnp.concatenate(
        [token(keys, t) * jnp.exp(final - cumulative[t]) for t in range(span)], axis=0
    )
    all_updates = jnp.concatenate(updates, axis=0).astype(BF16)
    decay_all = jnp.exp(final)
    for h in range(heads):
        cols = slice(h * size, (h + 1) * size)
        rank = lax.dot_general(
            blocked(tails[:, cols]),
            all_updates[:, cols],
            (((0,), (0,)), ((), ())),
            preferred_element_type=F32,
        )
        for n in range(seqs):
            state[n, :, cols] = (
                state[n, :, cols] * decay_all[n : n + 1, cols] + rank[n * size : (n + 1) * size, :]
            )
    write_state = pltpu.make_async_copy(state, new_state_hbm, store_sem.at[0])
    write_state.start()

    kv_gather_finish(0, head_all, own, far)
    heads_every = head_all[...].reshape(slots, vw)
    packed = dot(picker_kv, heads_every).astype(BF16)
    loads[6].wait()
    part = dot(packed, w_out[...])
    own_cols = tokens_ref.shape[1]

    def tp_scatter_start(phase, part, part_ref, recv_ref, group):
        for j in range(n_tp):
            part_ref[j, group, :] = part[group, j * own_cols : (j + 1) * own_cols].astype(BF16)
        copies = tp_copies(
            phase,
            lambda peer, d: part_ref.at[peer, group, :],
            lambda peer, d: recv_ref.at[d - 1, group, :],
        )
        exchange_start(copies)
        return copies

    def tp_scatter_finish(copies, part_ref, recv_ref, group):
        exchange_wait(copies)
        total = part_ref[tp, group, :].astype(F32)
        for d in range(1, n_tp):
            total = total + recv_ref[d - 1, group, :].astype(F32)
        return total

    cut = packs // 32 * 16
    groups = (slice(0, cut), slice(cut, packs))
    scatters = [
        tp_scatter_start((1, 4)[i], part, attn_part, attn_recv, group)
        for i, group in enumerate(groups)
    ]
    gathers = []
    for i, group in enumerate(groups):
        middle = (
            own_tokens[group, :] + tp_scatter_finish(scatters[i], attn_part, attn_recv, group)
        ).astype(BF16)
        mid_all[tp, group, :] = middle
        gathers.append(
            tp_copies(
                (2, 5)[i],
                lambda peer, d: mid_all.at[tp, group, :],
                lambda peer, d: mid_all.at[tp, group, :],
            )
        )
        exchange_start(gathers[-1])
    for copies in gathers:
        exchange_wait(copies)
    middle_rows = jnp.concatenate([mid_all[j] for j in range(n_tp)], axis=1).astype(F32)
    squares = jnp.sum(middle_rows * middle_rows, axis=1, keepdims=True)
    normed_mid = (middle_rows * mix_gain_ref[...]).astype(BF16)
    ff_pad = gu_part.shape[2]
    pad = ff_pad - ff
    empty = rows - packs
    if empty:
        normed_mid = jnp.concatenate([normed_mid, jnp.zeros((empty, width), BF16)], axis=0)
        squares = jnp.concatenate([squares, jnp.zeros((empty, 1), F32)], axis=0)
    square_high, square_low = high_low(squares)
    half = chips * unit
    normed_ref[...] = normed_mid
    side_ref[...] = jnp.concatenate(
        [square_high, square_low, jnp.zeros((rows, pad - 2), F32)], axis=1
    )
    middle_col = ff_pad // 256 * 128
    last_col = ff // 128 * 128
    gu_chunks = (
        (0, last_col, ff_pad),
        (0, 0, middle_col),
        (1, 0, middle_col),
        (0, middle_col, last_col),
        (1, middle_col, ff_pad),
    )

    def gu_chunk(index, c):
        m, low, high = gu_chunks[index]
        part = halves(c, half)
        stop = min(high, ff)
        weights = (w_gate, w_up)[m]
        if stop > low:
            gu_part[m, part, low:stop] = dot_t(normed_ref[part, :], weights[low:stop, :]).astype(
                BF16
            )
        if high > ff:
            side = side_ref[part, :] if m == 0 else jnp.zeros((half, pad), F32)
            gu_part[m, part, ff:high] = side.astype(BF16)

    def gu_finish(index):
        gu_pairs[index].wait()
        m, low, high = gu_chunks[index]
        cols = slice(low, high)
        for d in range(1, chips):
            dest = chip_at(d)
            at = halves(dest, unit)
            mine = pl.ds(pl.multiple_of(core * half + dest * unit, unit), unit)
            gu_red[m, d - 1, :, cols] = (
                gu_part[m, mine, cols].astype(F32) + gu_pair[m, at, cols].astype(F32)
            ).astype(BF16)
            gu_far[index].append(
                chip_start(
                    3 + index, d, gu_red.at[m, d - 1, :, cols], gu_recv.at[m, d - 1, :, cols]
                )
            )

    gu_pairs, gu_far = [], [[] for _ in gu_chunks]
    loads[7].wait()
    loads[8].wait()
    for index, (m, low, high) in enumerate(gu_chunks):
        gu_chunk(index, other)
        gu_pairs.append(
            pair_start(
                3 + index,
                gu_part.at[m, halves(other, half), slice(low, high)],
                gu_pair.at[m, :, slice(low, high)],
            )
        )
        gu_chunk(index, core)
        if index > 0:
            gu_finish(index - 1)
    gu_finish(len(gu_chunks) - 1)
    at = halves(chip, unit)
    mine = pl.ds(pl.multiple_of(core * half + chip * unit, unit), unit)

    def gu_sum(index):
        exchange_wait(gu_far[index])
        m, low, high = gu_chunks[index]
        cols = slice(low, high)
        total = gu_part[m, mine, cols].astype(F32) + gu_pair[m, at, cols].astype(F32)
        for d in range(1, chips):
            total = total + gu_recv[m, d - 1, :, cols].astype(F32)
        return total

    spot = core * chips + chip
    gate_last = gu_sum(0)
    lane = iota(gate_last.shape, 1) + last_col
    sq_mid = jnp.sum(
        jnp.where((lane == ff) | (lane == ff + 1), gate_last, 0.0), axis=1, keepdims=True
    )
    mid_scale = lax.rsqrt(sq_mid / D + EPSILON)
    gate_last = jnp.where(lane < ff, gate_last, 0.0)

    def hidden_of(gate, up):
        gate = gate * mid_scale
        return (gate / (1.0 + jnp.exp(-gate)) * (up * mid_scale)).astype(BF16)

    hid_first[spot] = hidden_of(gu_sum(1), gu_sum(2))
    own_first, far_first = kv_gather_start(1, hid_first)
    gate = jnp.concatenate([gu_sum(3), gate_last], axis=1)
    hid_second[spot] = hidden_of(gate, gu_sum(4))
    own_second, far_second = kv_gather_start(2, hid_second)
    kv_gather_finish(1, hid_first, own_first, far_first)
    loads[9].wait()
    hidden_all = hid_first[...].reshape(rows, middle_col)[0:packs, :]
    part = dot(hidden_all, w_down[0:middle_col, :])
    kv_gather_finish(2, hid_second, own_second, far_second)
    hidden_all = hid_second[...].reshape(rows, ff_pad - middle_col)[0:packs, 0 : ff - middle_col]
    part = part + dot(hidden_all, w_down[middle_col:ff, :])
    every = slice(0, packs)
    copies = tp_scatter_start(3, part, down_part, down_recv, every)
    down = tp_scatter_finish(copies, down_part, down_recv, every)
    result = (mid_all[tp].astype(F32) + down).astype(BF16)
    mixed_ref[...] = lax.dot_general(
        picker, result, (((0,), (0,)), ((), ())), preferred_element_type=F32
    ).astype(BF16)
    write_state.wait()


def fused_layer(n_kv, n_tp, *args):
    tokens, lengths, state, attn_gain, w_query = args[:5]
    w_beta, w_out, w_gate = args[7], args[12], args[14]
    batch, span, own_cols = tokens.shape
    seqs, size, vw = state.shape
    heads = vw // size
    width = attn_gain.shape[0]
    ff = w_gate.shape[1]
    pack = min(batch * 7 // 4, batch * span)
    unit = (pack + n_kv - 1) // n_kv
    unit = (unit + 15) // 16 * 16
    packs = (pack + 15) // 16 * 16
    rows = unit * n_kv
    local = seqs * span
    chips = n_kv // 2
    ff_pad = (ff + 2 + 127) // 128 * 128
    qkv_width = 3 * vw + 128
    dims = (n_kv, n_tp, batch, span, seqs, heads, size, width, ff, rows, packs, unit)
    operands = list(args)
    operands[0] = tokens.reshape(batch * span, own_cols)
    for at in (1, 3, 9, 10, 11, 13):
        operands[at] = operands[at].reshape(1, -1)
    for at in (7, 8, 14, 15):
        operands[at] = operands[at].T
    in_vmem = pl.BlockSpec(memory_space=pltpu.VMEM)
    in_hbm = pl.BlockSpec(memory_space=pl.ANY)
    vmem_args = (0, 1, 3, 9, 10, 11, 13)
    dma = pltpu.SemaphoreType.DMA

    def buf(*shape):
        return pltpu.VMEM(shape, BF16)

    mixed, new_state = pl.pallas_call(
        lambda *refs: layer_kernel(dims, *refs),
        out_shape=(
            jax.ShapeDtypeStruct((batch * span, own_cols), BF16),
            jax.ShapeDtypeStruct(state.shape, F32),
        ),
        in_specs=[in_vmem if i in vmem_args else in_hbm for i in range(len(operands))],
        out_specs=(in_vmem, in_hbm),
        scratch_shapes=[
            pltpu.VMEM(state.shape, F32),
            buf(3, width, vw),
            buf(w_beta.shape[1], width),
            buf(w_beta.shape[1], width),
            buf(*w_out.shape),
            buf(ff, width),
            buf(ff, width),
            buf(ff, w_out.shape[1]),
            buf(n_tp, packs, own_cols),
            buf(n_kv * local, qkv_width),
            buf(chips * local, qkv_width),
            buf(chips - 1, local, qkv_width),
            buf(chips - 1, local, qkv_width),
            buf(n_kv, local, vw),
            buf(n_tp, packs, own_cols),
            buf(n_tp - 1, packs, own_cols),
            buf(n_tp, packs, own_cols),
            buf(2, rows, ff_pad),
            buf(2, chips * unit, ff_pad),
            buf(2, chips - 1, unit, ff_pad),
            buf(2, chips - 1, unit, ff_pad),
            buf(n_kv, unit, ff_pad // 256 * 128),
            buf(n_kv, unit, ff_pad - ff_pad // 256 * 128),
            buf(n_tp, packs, own_cols),
            buf(n_tp - 1, packs, own_cols),
            buf(n_kv * local, width),
            buf(n_kv * local, 2),
            buf(rows, width),
            pltpu.VMEM((rows, ff_pad - ff), F32),
            dma((10,)),
            dma((1,)),
            dma((6, n_tp - 1)),
            dma((6, n_tp - 1)),
            dma((8,)),
            dma((8,)),
            dma((11, chips - 1)),
            dma((11, chips - 1)),
            dma((3, chips)),
            dma((3, chips)),
        ],
        compiler_params=pltpu.CompilerParams(
            collective_id=0, has_side_effects=True, vmem_limit_bytes=60 * 1024 * 1024
        ),
    )(*operands)
    count = state.shape[0]
    return pl.pallas_call(
        finish_kernel,
        out_shape=(
            jax.ShapeDtypeStruct(tokens.shape, BF16),
            jax.ShapeDtypeStruct(state.shape, F32),
        ),
        in_specs=[in_vmem, in_hbm],
        out_specs=(in_vmem, in_hbm),
        scratch_shapes=[pltpu.VMEM(state.shape, F32), dma((count,)), dma((count,))],
        compiler_params=pltpu.CompilerParams(vmem_limit_bytes=60 * 1024 * 1024),
    )(mixed, new_state)


def finish_kernel(mixed_ref, state_hbm, mixed_out, state_out, buffer, read_sem, write_sem):
    count = buffer.shape[0]
    reads = [
        pltpu.make_async_copy(state_hbm.at[n], buffer.at[n], read_sem.at[n]) for n in range(count)
    ]
    writes = [
        pltpu.make_async_copy(buffer.at[n], state_out.at[n], write_sem.at[n]) for n in range(count)
    ]
    for read in reads:
        read.start()
    mixed_out[...] = mixed_ref[...].astype(F32).reshape(mixed_out.shape).astype(BF16)
    for read, write in zip(reads, writes):
        read.wait()
        write.start()
    for write in writes:
        write.wait()


def layer(*args):
    n_kv, n_tp = lax.axis_size("kv"), lax.axis_size("tp")
    tokens, state = args[0], args[2]
    batch, span, own_cols = tokens.shape
    seqs, size, vw = state.shape
    aligned = own_cols % 128 == 0 and size % 128 == 0 and seqs == 8
    aligned = aligned and n_kv % 2 == 0 and 2 * args[7].shape[1] + 2 <= 128
    if aligned:
        return fused_layer(n_kv, n_tp, *args)
    return body(*args)


def solution(mesh):
    return jax.shard_map(
        layer,
        mesh=mesh,
        in_specs=(
            P(None, None, ("kv", "tp")),
            P(),
            P("kv", None, "tp"),
            P("kv"),
            P("kv", "tp"),
            P("kv", "tp"),
            P("kv", "tp"),
            P(),
            P(),
            P(),
            P(),
            P(),
            P("tp", "kv"),
            P("kv"),
            P("kv", "tp"),
            P("kv", "tp"),
            P("tp", "kv"),
        ),
        out_specs=(P(None, None, ("kv", "tp")), P("kv", None, "tp")),
        check_vma=False,
    )
```

profile of v0, /device:TPU:0, one launch (start us, length us, event | category | flops | bytes accessed | tf_op | source)
XLA Modules:
  0.0 70.2 jit_solution(10124595048480249610)
XLA Ops:
  0.6 64.5 %shard_map.176 = (bf16[256,128]{1,0:T(8,128)(2,1)}, f32[8,128,1024]{2,1,0:T(8,128)}) custom-call(bf16[256,128]{1,0:T(8,128)(2,1)} %bitcast.15, s32[1,64]{1,0:T(1,128)} %bitcast.18, f32[8,128,1024]{2,1,0:T(8,128)} %refs_2_.1, f32[1,512]{1,0:T(1,128)} %bitcast.16, bf16[512,1024]{1,0:T(8,128)(2,1)} %refs_4_.1, bf16[512,1024]{1,0:T(8,128)(2,1)} %refs_5_.1, ...), custom_call_target="tpu_custom_call" | custom-call | tf_op jit(solution)/shard_map/pallas_call | solution.py:825
  65.2 5.0 %shard_map.177 = (bf16[64,4,128]{2,1,0:T(4,128)(2,1)}, f32[8,128,1024]{2,1,0:T(8,128)}) custom-call(bf16[256,128]{1,0:T(8,128)(2,1)} %get-tuple-element.4.mixed_ref, f32[8,128,1024]{2,1,0:T(8,128)} %get-tuple-element.5.state_hbm), custom_call_target="tpu_custom_call" | custom-call | tf_op jit(solution)/shard_map/pallas_call | solution.py:879
where the time goes:
time: 70.4 us; the launch traced here: 70.2 us
  Pallas kernels  69.6 us (99%)
    pallas_call x1, Pallas kernels, fused_layer(): pl.pallas_call(lambda *refs: layer_kernel(dims, *refs), out_shape=(jax.Sh...  64.5 us
    pallas_call x1, Pallas kernels, fused_layer(): pl.pallas_call(finish_kernel, out_shape=(jax.ShapeDtypeStruct(tokens.shap...  5.05 us

commit v1 on v0

--- a/solution.py
+++ b/solution.py
@@ -221,26 +221,32 @@
 
 def layer_kernel(
     dims,
-    tokens_ref,
-    lengths_ref,
+    tokens_hbm,
+    lengths_hbm,
     state_hbm,
-    attn_gain_ref,
+    attn_gain_hbm,
     wq_hbm,
     wk_hbm,
     wv_hbm,
     wb_hbm,
     wa_hbm,
-    rate_ref,
-    bias_ref,
-    out_gain_ref,
+    rate_hbm,
+    bias_hbm,
+    out_gain_hbm,
     wo_hbm,
-    mix_gain_ref,
+    mix_gain_hbm,
     wg_hbm,
     wu_hbm,
     wd_hbm,
     mixed_ref,
-    new_state_hbm,
     state,
+    tokens_ref,
+    lengths_ref,
+    attn_gain_ref,
+    rate_ref,
+    bias_ref,
+    out_gain_ref,
+    mix_gain_ref,
     w_qkv,
     w_beta,
     w_alpha,
@@ -270,7 +276,7 @@
     normed_ref,
     side_ref,
     load_sem,
-    store_sem,
+    small_sem,
     tp_send,
     tp_recv,
     pair_send,
@@ -298,6 +304,33 @@
     def chip_from(d):
         return lax.rem(chip + chips - d, chips)
 
+    barrier = pltpu.get_barrier_semaphore()
+    pl.semaphore_signal(barrier, inc=1, device_id={"kv": partner}, device_id_type=MESH)
+    for d in range(1, chips):
+        pl.semaphore_signal(
+            barrier, inc=1, device_id={"kv": chip_at(d) * 2 + core}, device_id_type=MESH
+        )
+    for d in range(1, n_tp):
+        pl.semaphore_signal(
+            barrier, inc=1, device_id={"tp": lax.rem(tp + d, n_tp)}, device_id_type=MESH
+        )
+
+    smalls = [
+        pltpu.make_async_copy(source, dest, small_sem.at[i])
+        for i, (source, dest) in enumerate(
+            (
+                (tokens_hbm, tokens_ref),
+                (lengths_hbm, lengths_ref),
+                (attn_gain_hbm, attn_gain_ref),
+                (rate_hbm, rate_ref),
+                (bias_hbm, bias_ref),
+                (out_gain_hbm, out_gain_ref),
+                (mix_gain_hbm, mix_gain_ref),
+            )
+        )
+    ]
+    for load in smalls:
+        load.start()
     loads = [
         pltpu.make_async_copy(wq_hbm, w_qkv.at[0], load_sem.at[0]),
         pltpu.make_async_copy(wk_hbm, w_qkv.at[1], load_sem.at[1]),
@@ -317,17 +350,8 @@
     for load in loads:
         load.start()
 
-    barrier = pltpu.get_barrier_semaphore()
-    pl.semaphore_signal(barrier, inc=1, device_id={"kv": partner}, device_id_type=MESH)
-    for d in range(1, chips):
-        pl.semaphore_signal(
-            barrier, inc=1, device_id={"kv": chip_at(d) * 2 + core}, device_id_type=MESH
-        )
-    for d in range(1, n_tp):
-        pl.semaphore_signal(
-            barrier, inc=1, device_id={"tp": lax.rem(tp + d, n_tp)}, device_id_type=MESH
-        )
-
+    for load in smalls:
+        load.wait()
     lengths_row = lengths_ref[...].astype(F32)
     spread = (iota((batch, slots), 1) // span == iota((batch, slots), 0)).astype(BF16)
     length_of = dot(jnp.broadcast_to(lengths_row, (8, batch)).astype(BF16), spread)
@@ -622,8 +646,6 @@
             state[n, :, cols] = (
                 state[n, :, cols] * decay_all[n : n + 1, cols] + rank[n * size : (n + 1) * size, :]
             )
-    write_state = pltpu.make_async_copy(state, new_state_hbm, store_sem.at[0])
-    write_state.start()
 
     kv_gather_finish(0, head_all, own, far)
     heads_every = head_all[...].reshape(slots, vw)
@@ -787,7 +809,6 @@
     mixed_ref[...] = lax.dot_general(
         picker, result, (((0,), (0,)), ((), ())), preferred_element_type=F32
     ).astype(BF16)
-    write_state.wait()
 
 
 def fused_layer(n_kv, n_tp, *args):
@@ -815,8 +836,7 @@
     for at in (7, 8, 14, 15):
         operands[at] = operands[at].T
     in_vmem = pl.BlockSpec(memory_space=pltpu.VMEM)
-    in_hbm = pl.BlockSpec(memory_space=pl.ANY)
-    vmem_args = (0, 1, 3, 9, 10, 11, 13)
+    in_hbm = pl.BlockSpec(memory_space=pltpu.HBM)
     dma = pltpu.SemaphoreType.DMA
 
     def buf(*shape):
@@ -825,13 +845,19 @@
     mixed, new_state = pl.pallas_call(
         lambda *refs: layer_kernel(dims, *refs),
         out_shape=(
-            jax.ShapeDtypeStruct((batch * span, own_cols), BF16),
-            jax.ShapeDtypeStruct(state.shape, F32),
+            pltpu.VMEM((batch * span, own_cols), BF16),
+            pltpu.VMEM(state.shape, F32),
         ),
-        in_specs=[in_vmem if i in vmem_args else in_hbm for i in range(len(operands))],
-        out_specs=(in_vmem, in_hbm),
+        in_specs=[in_hbm] * len(operands),
+        out_specs=(in_vmem, in_vmem),
         scratch_shapes=[
-            pltpu.VMEM(state.shape, F32),
+            buf(batch * span, own_cols),
+            pltpu.VMEM((1, batch), jnp.int32),
+            pltpu.VMEM((1, width), F32),
+            pltpu.VMEM((1, args[9].shape[0]), F32),
+            pltpu.VMEM((1, args[10].shape[0]), F32),
+            pltpu.VMEM((1, size), F32),
+            pltpu.VMEM((1, width), F32),
             buf(3, width, vw),
             buf(w_beta.shape[1], width),
             buf(w_beta.shape[1], width),
@@ -861,7 +887,7 @@
             buf(rows, width),
             pltpu.VMEM((rows, ff_pad - ff), F32),
             dma((10,)),
-            dma((1,)),
+            dma((7,)),
             dma((6, n_tp - 1)),
             dma((6, n_tp - 1)),
             dma((8,)),
@@ -872,7 +898,7 @@
             dma((3, chips)),
         ],
         compiler_params=pltpu.CompilerParams(
-            collective_id=0, has_side_effects=True, vmem_limit_bytes=60 * 1024 * 1024
+            collective_id=0, has_side_effects=True, vmem_limit_bytes=52 * 1024 * 1024
         ),
     )(*operands)
     count = state.shape[0]
@@ -882,27 +908,24 @@
             jax.ShapeDtypeStruct(tokens.shape, BF16),
             jax.ShapeDtypeStruct(state.shape, F32),
         ),
-        in_specs=[in_vmem, in_hbm],
-        out_specs=(in_vmem, in_hbm),
-        scratch_shapes=[pltpu.VMEM(state.shape, F32), dma((count,)), dma((count,))],
-        compiler_params=pltpu.CompilerParams(vmem_limit_bytes=60 * 1024 * 1024),
+        in_specs=[in_vmem, in_vmem],
+        out_specs=(in_hbm, in_hbm),
+        scratch_shapes=[pltpu.VMEM(tokens.shape, BF16), dma((count + 1,))],
+        compiler_params=pltpu.CompilerParams(vmem_limit_bytes=8 * 1024 * 1024),
     )(mixed, new_state)
 
 
-def finish_kernel(mixed_ref, state_hbm, mixed_out, state_out, buffer, read_sem, write_sem):
-    count = buffer.shape[0]
-    reads = [
-        pltpu.make_async_copy(state_hbm.at[n], buffer.at[n], read_sem.at[n]) for n in range(count)
+def finish_kernel(mixed_ref, state_ref, mixed_out, state_out, mixed_rows, write_sem):
+    count = state_ref.shape[0]
+    writes = [
+        pltpu.make_async_copy(state_ref.at[n], state_out.at[n], write_sem.at[n])
+        for n in range(count)
     ]
-    writes = [
-        pltpu.make_async_copy(buffer.at[n], state_out.at[n], write_sem.at[n]) for n in range(count)
-    ]
-    for read in reads:
-        read.start()
-    mixed_out[...] = mixed_ref[...].astype(F32).reshape(mixed_out.shape).astype(BF16)
-    for read, write in zip(reads, writes):
-        read.wait()
+    for write in writes:
         write.start()
+    mixed_rows[...] = mixed_ref[...].astype(F32).reshape(mixed_rows.shape).astype(BF16)
+    writes.append(pltpu.make_async_copy(mixed_rows, mixed_out, write_sem.at[count]))
+    writes[-1].start()
     for write in writes:
         write.wait()
 

time: 70.4 us -> 69.1 us (0.982)
  Pallas kernels: 69.6 us -> 68.3 us
    pallas_call x1, Pallas kernels: 5.05 us -> 2.09 us  [fused_layer(): pl.pallas_call(finish_kernel, out_shape=(jax.ShapeDtypeStruct(tokens.shap...]
    pallas_call x1, Pallas kernels: 64.5 us -> 66.2 us  [fused_layer(): pl.pallas_call(lambda *refs: layer_kernel(dims, *refs), out_shape=(pltpu....]
where the time goes in v1:
time: 69.1 us; the launch traced here: 68.9 us
  Pallas kernels  68.3 us (99%)
    pallas_call x1, Pallas kernels, fused_layer(): pl.pallas_call(lambda *refs: layer_kernel(dims, *refs), out_shape=(pltpu....  66.2 us
    pallas_call x1, Pallas kernels, fused_layer(): pl.pallas_call(finish_kernel, out_shape=(jax.ShapeDtypeStruct(tokens.shap...  2.09 us

profile of v1, /device:TPU:0, one launch (start us, length us, event | category | flops | bytes accessed | tf_op | source)
XLA Modules:
  0.0 68.9 jit_solution(12843769052723326900)
XLA Ops:
  0.6 66.2 %shard_map.176 = (bf16[256,128]{1,0:T(8,128)(2,1)S(1)}, f32[8,128,1024]{2,1,0:T(8,128)S(1)}) custom-call(bf16[256,128]{1,0:T(8,128)(2,1)} %bitcast.15, s32[1,64]{1,0:T(1,128)} %bitcast.18, f32[8,128,1024]{2,1,0:T(8,128)} %refs_2_.1, f32[1,512]{1,0:T(1,128)} %bitcast.16, bf16[512,1024]{1,0:T(8,128)(2,1)} %refs_4_.1, bf16[512,1024]{1,0:T(8,128)(2,1)} %refs_5_.1, ...), custom_call_target="tpu_custom_call" | custom-call | tf_op jit(solution)/shard_map/pallas_call | solution.py:845
  66.8 2.1 %shard_map.177 = (bf16[64,4,128]{2,1,0:T(4,128)(2,1)}, f32[8,128,1024]{2,1,0:T(8,128)}) custom-call(bf16[256,128]{1,0:T(8,128)(2,1)S(1)} %get-tuple-element.4.mixed_ref, f32[8,128,1024]{2,1,0:T(8,128)S(1)} %get-tuple-element.5.state_ref), custom_call_target="tpu_custom_call" | custom-call | tf_op jit(solution)/shard_map/pallas_call | solution.py:905
